TPU v7x, 32 devices: a whole 2x2x4 slice. The times are simulated.
32 devices in a mesh: sp: 4 (over y, x), tp: 8 (over z, core).
Axes of the slice: x: 2, y: 2, z: 4, core: 2. Of those that a mesh axis runs over, the one named last changes fastest.
Arguments:
- stream: bfloat16 [2048, 1024], P('sp', 'tp'), may hold values from -6 to 6
- gain_first: bfloat16 [1024], P('tp'), may hold values from 0.099609375 to 1.8984375
- query_first: bfloat16 [1024, 1024], P('sp', 'tp'), may hold values from -0.1875 to 0.1875
- key_first: bfloat16 [1024, 1024], P('sp', 'tp'), may hold values from -0.1875 to 0.1875
- value_first: bfloat16 [1024, 1024], P('sp', 'tp'), may hold values from -0.1875 to 0.1875
- offset_first: float32 [8, 15, 31], P('tp'), may hold values from -4 to 254
- gain_second: bfloat16 [1024], P('tp'), may hold values from 0.099609375 to 1.8984375
- query_second: bfloat16 [1024, 1024], P('sp', 'tp'), may hold values from -0.1875 to 0.1875
- key_second: bfloat16 [1024, 1024], P('sp', 'tp'), may hold values from -0.1875 to 0.1875
- value_second: bfloat16 [1024, 1024], P('sp', 'tp'), may hold values from -0.1875 to 0.1875
- offset_second: float32 [8, 15, 31], P('tp'), may hold values from -4 to 254
Outputs:
- result: bfloat16 [2048, 1024], P('sp', 'tp')
All inputs are finite; a program needn't handle non-finite values.
Results may differ from a plain program's by a relative error of at most 0.008.
Values may be sent and summed in bfloat16 or wider, within the bound.
A program may use at most 64 MiB of HBM per device.

v0:
```python
import jax
import jax.numpy as jnp
import numpy as np
from jax import lax
from jax.sharding import PartitionSpec as P

GRID_W = 64


epsilon = 1e-06


def padded_2(block, sides, width):
    for axis, dim in sides:
        count = lax.axis_size(axis)
        forward = [(i, i + 1) for i in range(count - 1)]
        backward = [(target, source) for source, target in forward]
        low = lax.ppermute(
            lax.slice_in_dim(block, block.shape[dim] - width, None, axis=dim), axis, forward
        )
        high = lax.ppermute(lax.slice_in_dim(block, 0, width, axis=dim), axis, backward)
        block = jnp.concatenate([low, block, high], axis=dim)
    return block


def attend(query, keys, values, table, row_start, total_rows):
    rows_here, width, heads, head_size = query.shape
    blocks = width // 16
    query_cols = np.arange(width).reshape(blocks, 16)
    window_start = np.clip(query_cols - 8, 0, width - 16)
    key_cols = np.clip(np.arange(blocks) * 16 - 8, 0, width - 32)[:, None] + np.arange(32)
    column_ok = (key_cols[:, None, :] >= window_start[:, :, None]) & (
        key_cols[:, None, :] < window_start[:, :, None] + 16
    )
    column_offset = np.clip(key_cols[:, None, :] - query_cols[:, :, None] + 15, 0, 30)
    column_bias = table[:, :, column_offset]
    mask = jnp.asarray(column_ok)[None, :, :, None, :]
    factor = head_size ** (-0.5)

    def one_row(index):
        grid_row = row_start + index
        first = jnp.clip(grid_row - 4, 0, total_rows - 8)
        local = first - row_start + 4
        key_block = lax.dynamic_slice_in_dim(keys, local, 8, 0)[:, key_cols]
        value_block = lax.dynamic_slice_in_dim(values, local, 8, 0)[:, key_cols]
        query_row = lax.dynamic_index_in_dim(query, index, 0, keepdims=False).reshape(
            blocks, 16, heads, head_size
        )
        scores = (
            jnp.einsum(
                "jqhe,mjkhe->hjqmk", query_row, key_block, preferred_element_type=jnp.float32
            )
            * factor
        )
        row_offset = first + jnp.arange(8, dtype=jnp.int32) - grid_row + 7
        row_bias = jnp.transpose(jnp.take(column_bias, row_offset, axis=1), (0, 2, 3, 1, 4))
        scores = jnp.where(mask, scores + row_bias, -1e30)
        weight = jax.nn.softmax(scores.reshape(heads, blocks, 16, 256), axis=-1)
        rounded = weight.astype(jnp.bfloat16).reshape(heads, blocks, 16, 8, 32)
        output = jnp.einsum(
            "hjqmk,mjkhe->jqhe", rounded, value_block, preferred_element_type=jnp.float32
        )
        return output.reshape(width, heads * head_size)

    return jax.vmap(one_row)(jnp.arange(rows_here, dtype=jnp.int32))


def layer(stream, gain, w_query, w_key, w_value, table):
    tokens_dev, local_width = stream.shape
    widened = stream.astype(jnp.float32)
    full_rows, full_gain = (
        lax.all_gather(stream, "tp", axis=1, tiled=True),
        lax.all_gather(gain, "tp", axis=0, tiled=True),
    )
    full_wide = full_rows.astype(jnp.float32)
    mean_square = jnp.mean(full_wide * full_wide, axis=-1, keepdims=True)
    normed = (full_wide * lax.rsqrt(mean_square + epsilon) * full_gain.astype(jnp.float32)).astype(
        jnp.bfloat16
    )
    pieces = (
        lax.all_gather(w_query, "sp", axis=0, tiled=True),
        lax.all_gather(w_key, "sp", axis=0, tiled=True),
        lax.all_gather(w_value, "sp", axis=0, tiled=True),
    )
    query, key_part, value_part = tuple(
        (jnp.dot(normed, piece, preferred_element_type=jnp.float32) for piece in pieces)
    )
    heads_dev = table.shape[0]
    rows_dev = tokens_dev // GRID_W
    shape = (rows_dev, GRID_W, heads_dev, local_width // heads_dev)
    query = query.astype(jnp.bfloat16).reshape(shape)
    paired = jnp.stack(
        [
            key_part.astype(jnp.bfloat16).reshape(shape),
            value_part.astype(jnp.bfloat16).reshape(shape),
        ]
    )
    padded = padded_2(paired, (("sp", 1),), 4)
    row_start = lax.axis_index("sp") * rows_dev
    output = attend(query, padded[0], padded[1], table, row_start, rows_dev * lax.axis_size("sp"))
    return (widened + output.reshape(tokens_dev, local_width)).astype(jnp.bfloat16)


def body(
    stream,
    gain_first,
    query_first,
    key_first,
    value_first,
    offset_first,
    gain_second,
    query_second,
    key_second,
    value_second,
    offset_second,
):
    middle = layer(stream, gain_first, query_first, key_first, value_first, offset_first)
    return layer(middle, gain_second, query_second, key_second, value_second, offset_second)


def solution(mesh):
    placed = (
        P("sp", "tp"),
        P("tp"),
        P("sp", "tp"),
        P("sp", "tp"),
        P("sp", "tp"),
        P("tp", None, None),
        P("tp"),
        P("sp", "tp"),
        P("sp", "tp"),
        P("sp", "tp"),
        P("tp", None, None),
    )
    return jax.shard_map(body, mesh=mesh, in_specs=placed, out_specs=P("sp", "tp"), check_vma=False)
```

profile of v0, /device:TPU:0, one launch (start us, length us, event | category | flops | bytes accessed | tf_op | source)
XLA Modules:
  0.0 178.0 jit_solution(1198748897134902003)
XLA Ops:
  7.3 13.6 %all-gather = bf16[8,1,128]{2,1,0:T(2,128)(2,1)S(1)} all-gather(bf16[1,1,128]{2,1,0:T(2,128)(2,1)} %bitcast.156), channel_id=1, replica_groups=mesh['sp'=4,'tp'=8] {'tp'}, dimensions={0}, use_global_device_ids=true | all-gather | bytes 2304 | tf_op jit(solution)/shard_map/all_gather | solution.py:73
  22.6 5.5 %gather_fusion.5 = f32[2048,15]{1,0:T(8,128)S(1)} fusion(f32[15,31]{0,1:T(8,128)S(1)} %bitcast.126, s32[2048]{0:T(1024)S(1)} %broadcast_clamp_fusion), kind=kCustom, calls=%fused_computation.7 | custom fusion | bytes 253952 | tf_op jit(solution)/shard_map/gather | solution.py:36
  29.5 9.0 %all_gather.32 = bf16[1024,128]{1,0:T(8,128)(2,1)S(1)} all-gather(bf16[256,128]{1,0:T(8,128)(2,1)S(1)} %copy-done.4), channel_id=1, replica_groups=mesh['sp'=4,'tp'=8] {'sp'}, dimensions={0}, use_global_device_ids=true | all-gather | bytes 327680 | tf_op jit(solution)/shard_map/all_gather | solution.py:82
  38.5 9.0 %all_gather.33 = bf16[1024,128]{1,0:T(8,128)(2,1)S(1)} all-gather(bf16[256,128]{1,0:T(8,128)(2,1)S(1)} %copy-done.5), channel_id=1, replica_groups=mesh['sp'=4,'tp'=8] {'sp'}, dimensions={0}, use_global_device_ids=true | all-gather | bytes 327680 | tf_op jit(solution)/shard_map/all_gather | solution.py:83
  47.5 8.4 %all_gather.34 = bf16[1024,128]{1,0:T(8,128)(2,1)S(1)} all-gather(bf16[256,128]{1,0:T(8,128)(2,1)S(1)} %copy-done.6), channel_id=1, replica_groups=mesh['sp'=4,'tp'=8] {'sp'}, dimensions={0}, use_global_device_ids=true | all-gather | bytes 327680 | tf_op jit(solution)/shard_map/all_gather | solution.py:81
  61.0 3.0 %collective-permute-start = (bf16[2,4,64,1,128]{4,2,1,3,0:T(8,128)(2,1)S(1)}, bf16[2,4,64,1,128]{4,2,1,3,0:T(8,128)(2,1)S(1)}, u32[]{:S(2)}, u32[]{:S(2)}) collective-permute-start(bf16[2,4,64,1,128]{4,2,1,3,0:T(8,128)(2,1)S(1)} %get-tuple-element.12), channel_id=1, source_target_pairs={{0,8},{8,16},{16,24},{1,9},{9,17},{17,25},{2,10},{10,18},{18,26},{... | collective-permute-start | bytes 393224 | tf_op jit(solution)/shard_map/ppermute | solution.py:18
  66.6 4.4 %collective-permute-done.1 = bf16[2,4,64,1,128]{4,2,1,3,0:T(8,128)(2,1)S(1)} collective-permute-done((bf16[2,4,64,1,128]{4,2,1,3,0:T(8,128)(2,1)S(1)}, bf16[2,4,64,1,128]{4,2,1,3,0:T(8,128)(2,1)S(1)}, u32[]{:S(2)}, u32[]{:S(2)}) %collective-permute-start.1) | collective-permute-done | bytes 131104 | tf_op jit(solution)/shard_map/ppermute | solution.py:21
  72.7 1.9 %copy.56 = bf16[8,8,64,128]{3,1,2,0:T(8,128)(2,1)S(1)} copy(bf16[8,8,64,128]{3,2,1,0:T(8,128)(2,1)} %gather_fusion.3) | data formatting | bytes 2097152 | tf_op jit(solution)/shard_map/vmap()/gather | solution.py:44
  74.6 2.7 %gather_fusion.4 = bf16[128,8,8,128]{3,2,1,0:T(8,128)(2,1)} fusion(bf16[8,8,64,128]{3,1,2,0:T(8,128)(2,1)S(1)} %copy.56, s32[1024]{0:T(1024)} %pad_clamp_fusion.1), kind=kCustom, calls=%fused_computation.6 | custom fusion | bytes 4194816 | tf_op jit(solution)/shard_map/vmap()/gather | solution.py:44
  77.3 4.5 %fusion.39 = (f32[8,4,16]{2,1,0:T(4,128)S(1)}, f32[8,1,4,16,8,32]{5,3,4,2,0,1:T(8,128)S(1)}) fusion(f32[8,1,8,4,16,32]{5,4,3,2,0,1:T(8,128)S(1)} %bitcast.130, pred[8,8]{1,0:T(8,128)(4,1)} %compare_and_fusion, bf16[8,4,16,128,1]{3,2,4,1,0:T(8,128)(2,1)S(1)} %bitcast.139, bf16[4,32,8,8,128]{4,3,2,1,0:T(8,128)(2,1)} %bitcast.135, ...), kind=kOutput, calls=%fused_computation.87 | convolution fusion | flops 34209280 | bytes 3280960 | tf_op jit(solution)/shard_map/vmap(jqhe,mjkhe->hjqmk)/dot_general | solution.py:50
  87.8 2.5 %gather_fusion.1 = bf16[128,8,8,128]{3,2,1,0:T(8,128)(2,1)} fusion(bf16[8,8,64,128]{3,1,2,0:T(8,128)(2,1)S(1)} %copy.52, s32[1024]{0:T(1024)S(1)} %copy-done.10), kind=kCustom, calls=%fused_computation.3 | custom fusion | bytes 4194816 | tf_op jit(solution)/shard_map/vmap()/gather | solution.py:45
  90.4 2.4 %fusion.14 = f32[8,4,128,16,1]{2,3,4,1,0:T(8,128)S(1)} fusion(bf16[8,4,16,8,32]{2,3,4,1,0:T(8,128)(2,1)S(1)} %copy.61, bf16[4,32,8,8,128]{4,3,2,1,0:T(8,128)(2,1)} %bitcast.133), kind=kOutput, calls=%fused_computation.34 | convolution fusion | flops 33554432 | bytes 2621440 | tf_op jit(solution)/shard_map/vmap(hjqmk,mjkhe->jqhe)/dot_general | solution.py:60
  93.6 8.6 %all-gather.1 = bf16[8,1,128]{2,1,0:T(2,128)(2,1)S(1)} all-gather(bf16[1,1,128]{2,1,0:T(2,128)(2,1)S(1)} %bitcast.157), channel_id=1, replica_groups=mesh['sp'=4,'tp'=8] {'tp'}, dimensions={0}, use_global_device_ids=true | all-gather | bytes 2304 | tf_op jit(solution)/shard_map/all_gather | solution.py:73
  102.3 5.5 %gather_fusion.11 = f32[2048,15]{1,0:T(8,128)S(1)} fusion(f32[15,31]{0,1:T(8,128)S(1)} %bitcast.127, s32[2048]{0:T(1024)S(1)} %broadcast_clamp_fusion), kind=kCustom, calls=%fused_computation.13 | custom fusion | bytes 253952 | tf_op jit(solution)/shard_map/gather | solution.py:36
  109.2 9.8 %all_gather.38 = bf16[1024,128]{1,0:T(8,128)(2,1)S(1)} all-gather(bf16[256,128]{1,0:T(8,128)(2,1)S(1)} %copy-done.7), channel_id=1, replica_groups=mesh['sp'=4,'tp'=8] {'sp'}, dimensions={0}, use_global_device_ids=true | all-gather | bytes 327680 | tf_op jit(solution)/shard_map/all_gather | solution.py:83
  119.0 7.5 %all_gather.37 = bf16[1024,128]{1,0:T(8,128)(2,1)S(1)} all-gather(bf16[256,128]{1,0:T(8,128)(2,1)S(1)} %copy-done.8), channel_id=1, replica_groups=mesh['sp'=4,'tp'=8] {'sp'}, dimensions={0}, use_global_device_ids=true | all-gather | bytes 327680 | tf_op jit(solution)/shard_map/all_gather | solution.py:82
  126.5 9.5 %all_gather.39 = bf16[1024,128]{1,0:T(8,128)(2,1)S(1)} all-gather(bf16[256,128]{1,0:T(8,128)(2,1)S(1)} %copy-done.9), channel_id=1, replica_groups=mesh['sp'=4,'tp'=8] {'sp'}, dimensions={0}, use_global_device_ids=true | all-gather | bytes 327680 | tf_op jit(solution)/shard_map/all_gather | solution.py:81
  139.9 1.9 %collective-permute-start.2 = (bf16[2,4,64,1,128]{4,2,1,3,0:T(8,128)(2,1)S(1)}, bf16[2,4,64,1,128]{4,2,1,3,0:T(8,128)(2,1)S(1)}, u32[]{:S(2)}, u32[]{:S(2)}) collective-permute-start(bf16[2,4,64,1,128]{4,2,1,3,0:T(8,128)(2,1)S(1)} %get-tuple-element.10), channel_id=1, source_target_pairs={{0,8},{8,16},{16,24},{1,9},{9,17},{17,25},{2,10},{10,18},{18,26},{... | collective-permute-start | bytes 393224 | tf_op jit(solution)/shard_map/ppermute | solution.py:18
  144.3 4.4 %collective-permute-done.3 = bf16[2,4,64,1,128]{4,2,1,3,0:T(8,128)(2,1)S(1)} collective-permute-done((bf16[2,4,64,1,128]{4,2,1,3,0:T(8,128)(2,1)S(1)}, bf16[2,4,64,1,128]{4,2,1,3,0:T(8,128)(2,1)S(1)}, u32[]{:S(2)}, u32[]{:S(2)}) %collective-permute-start.3) | collective-permute-done | bytes 131104 | tf_op jit(solution)/shard_map/ppermute | solution.py:21
  150.5 1.9 %copy.66 = bf16[8,8,64,128]{3,1,2,0:T(8,128)(2,1)S(1)} copy(bf16[8,8,64,128]{3,2,1,0:T(8,128)(2,1)} %gather_fusion.9) | data formatting | bytes 2097152 | tf_op jit(solution)/shard_map/vmap()/gather | solution.py:44
  152.4 2.5 %gather_fusion.10 = bf16[128,8,8,128]{3,2,1,0:T(8,128)(2,1)} fusion(bf16[8,8,64,128]{3,1,2,0:T(8,128)(2,1)S(1)} %copy.66, s32[1024]{0:T(1024)S(1)} %copy-done.11), kind=kCustom, calls=%fused_computation.12 | custom fusion | bytes 4194816 | tf_op jit(solution)/shard_map/vmap()/gather | solution.py:44
  154.9 4.5 %fusion.40 = (f32[8,4,16]{2,1,0:T(4,128)S(1)}, f32[8,1,4,16,8,32]{5,3,4,2,0,1:T(8,128)S(1)}) fusion(f32[8,1,8,4,16,32]{5,4,3,2,0,1:T(8,128)S(1)} %bitcast.131, pred[8,8]{1,0:T(8,128)(4,1)S(1)} %copy-done.14, bf16[8,4,16,128,1]{3,2,4,1,0:T(8,128)(2,1)S(1)} %bitcast.138, bf16[4,32,8,8,128]{4,3,2,1,0:T(8,128)(2,1)} %bitcast.134, ...), kind=kOutput, calls=%fused_computation.88 | convolution fusion | flops 34209280 | bytes 3280960 | tf_op jit(solution)/shard_map/vmap(jqhe,mjkhe->hjqmk)/dot_general | solution.py:50
  165.4 2.5 %gather_fusion.7 = bf16[128,8,8,128]{3,2,1,0:T(8,128)(2,1)} fusion(bf16[8,8,64,128]{3,1,2,0:T(8,128)(2,1)S(1)} %copy.62, s32[1024]{0:T(1024)S(1)} %copy-done.11), kind=kCustom, calls=%fused_computation.9 | custom fusion | bytes 4194816 | tf_op jit(solution)/shard_map/vmap()/gather | solution.py:45
  168.0 2.4 %fusion.9 = f32[8,4,128,16,1]{2,3,4,1,0:T(8,128)S(1)} fusion(bf16[8,4,16,8,32]{2,3,4,1,0:T(8,128)(2,1)S(1)} %copy.71, bf16[4,32,8,8,128]{4,3,2,1,0:T(8,128)(2,1)} %bitcast.132), kind=kOutput, calls=%fused_computation.28 | convolution fusion | flops 33554432 | bytes 2621440 | tf_op jit(solution)/shard_map/vmap(hjqmk,mjkhe->jqhe)/dot_general | solution.py:60
  (95 shorter events, 36.1 us)
Async XLA Ops:
  6.5 50.6 %all-gather.5.cloned.1.call-start = ((), (), s32[]{:S(2)}) async-start(), calls=%async_computation | async-start | bytes 1179648 | tf_op jit(solution)/shard_map/all_gather | solution.py:72
  7.3 128.7 %all-gather.7.cloned.1.call-start = ((), (), s32[]{:S(2)}) async-start(), calls=%async_computation.1 | async-start | bytes 1179648 | tf_op jit(solution)/shard_map/all_gather | solution.py:72
  28.7 0.8 copy-start.12
  28.7 0.8 copy-start.4
  28.7 9.8 %copy-start.5 = (bf16[256,128]{1,0:T(8,128)(2,1)S(1)}, bf16[256,128]{1,0:T(8,128)(2,1)}, u32[]{:S(2)}) copy-start(bf16[256,128]{1,0:T(8,128)(2,1)} %param.29) | copy-start | bytes 196612
  28.7 18.8 %copy-start.6 = (bf16[256,128]{1,0:T(8,128)(2,1)S(1)}, bf16[256,128]{1,0:T(8,128)(2,1)}, u32[]{:S(2)}) copy-start(bf16[256,128]{1,0:T(8,128)(2,1)} %param.27) | copy-start | bytes 196612
  28.7 27.1 %copy-start.17 = (s32[128]{0:T(128)S(1)}, s32[128]{0:T(128)}, u32[]{:S(2)}) copy-start(s32[128]{0:T(128)} %constant.239) | copy-start | bytes 1540
  57.1 3.3 %copy-start.1 = (bf16[512,1024]{1,0:T(8,128)(2,1)S(1)}, bf16[512,1024]{1,0:T(8,128)(2,1)}, u32[]{:S(2)}) copy-start(bf16[512,1024]{1,0:T(8,128)(2,1)} %all-gather.5.cloned.1.call-done) | copy-start | bytes 3145732
  61.0 5.6 %collective-permute-start = (bf16[2,4,64,1,128]{4,2,1,3,0:T(8,128)(2,1)S(1)}, bf16[2,4,64,1,128]{4,2,1,3,0:T(8,128)(2,1)S(1)}, u32[]{:S(2)}, u32[]{:S(2)}) collective-permute-start(bf16[2,4,64,1,128]{4,2,1,3,0:T(8,128)(2,1)S(1)} %get-tuple-element.12), channel_id=1, source_target_pairs={{0,8},{8,16},{16,24},{1,9},{9,17},{17,25},{2,10},{10,18},{18,26},{... | collective-permute-start | bytes 393224 | tf_op jit(solution)/shard_map/ppermute | solution.py:18
  64.1 6.9 %collective-permute-start.1 = (bf16[2,4,64,1,128]{4,2,1,3,0:T(8,128)(2,1)S(1)}, bf16[2,4,64,1,128]{4,2,1,3,0:T(8,128)(2,1)S(1)}, u32[]{:S(2)}, u32[]{:S(2)}) collective-permute-start(bf16[2,4,64,1,128]{4,2,1,3,0:T(8,128)(2,1)S(1)} %get-tuple-element.13), channel_id=1, source_target_pairs={{8,0},{16,8},{24,16},{9,1},{17,9},{25,17},{10,2},{18,10},{26,18},{... | collective-permute-start | bytes 393224 | tf_op jit(solution)/shard_map/ppermute | solution.py:21
  84.2 3.6 %copy-start.10 = (s32[1024]{0:T(1024)S(1)}, s32[1024]{0:T(1024)}, u32[]{:S(2)}) copy-start(s32[1024]{0:T(1024)} %pad_clamp_fusion.1) | copy-start | bytes 12292
  90.4 2.4 %copy-start.3 = (bf16[512,128]{1,0:T(8,128)(2,1)S(1)}, bf16[512,128]{1,0:T(8,128)(2,1)}, u32[]{:S(2)}) copy-start(bf16[512,128]{1,0:T(8,128)(2,1)} %param.25) | copy-start | bytes 393220
  90.4 3.2 %copy-start.16 = (bf16[128]{0:T(256)(128)(2,1)S(1)}, bf16[128]{0:T(256)(128)(2,1)}, u32[]{:S(2)}) copy-start(bf16[128]{0:T(256)(128)(2,1)} %param.31) | copy-start | bytes 772
  90.4 11.8 %copy-start.15 = (f32[1,15,31]{2,0,1:T(1,128)S(1)}, f32[1,15,31]{2,0,1:T(1,128)}, u32[]{:S(2)}) copy-start(f32[1,15,31]{2,0,1:T(1,128)} %param.35) | copy-start | bytes 5584
  102.3 6.1 %copy-start.13 = (s32[1024]{0:T(1024)S(1)}, s32[1024]{0:T(1024)}, u32[]{:S(2)}) copy-start(s32[1024]{0:T(1024)} %copy-done.12) | copy-start | bytes 12292
  108.4 0.8 copy-start.7
  108.4 10.7 %copy-start.8 = (bf16[256,128]{1,0:T(8,128)(2,1)S(1)}, bf16[256,128]{1,0:T(8,128)(2,1)}, u32[]{:S(2)}) copy-start(bf16[256,128]{1,0:T(8,128)(2,1)} %param.33) | copy-start | bytes 196612
  108.4 18.1 %copy-start.9 = (bf16[256,128]{1,0:T(8,128)(2,1)S(1)}, bf16[256,128]{1,0:T(8,128)(2,1)}, u32[]{:S(2)}) copy-start(bf16[256,128]{1,0:T(8,128)(2,1)} %param.32) | copy-start | bytes 196612
  136.0 3.3 %copy-start.2 = (bf16[512,1024]{1,0:T(8,128)(2,1)S(1)}, bf16[512,1024]{1,0:T(8,128)(2,1)}, u32[]{:S(2)}) copy-start(bf16[512,1024]{1,0:T(8,128)(2,1)} %all-gather.7.cloned.1.call-done) | copy-start | bytes 3145732
  139.9 4.4 %collective-permute-start.2 = (bf16[2,4,64,1,128]{4,2,1,3,0:T(8,128)(2,1)S(1)}, bf16[2,4,64,1,128]{4,2,1,3,0:T(8,128)(2,1)S(1)}, u32[]{:S(2)}, u32[]{:S(2)}) collective-permute-start(bf16[2,4,64,1,128]{4,2,1,3,0:T(8,128)(2,1)S(1)} %get-tuple-element.10), channel_id=1, source_target_pairs={{0,8},{8,16},{16,24},{1,9},{9,17},{17,25},{2,10},{10,18},{18,26},{... | collective-permute-start | bytes 393224 | tf_op jit(solution)/shard_map/ppermute | solution.py:18
  141.8 6.9 %collective-permute-start.3 = (bf16[2,4,64,1,128]{4,2,1,3,0:T(8,128)(2,1)S(1)}, bf16[2,4,64,1,128]{4,2,1,3,0:T(8,128)(2,1)S(1)}, u32[]{:S(2)}, u32[]{:S(2)}) collective-permute-start(bf16[2,4,64,1,128]{4,2,1,3,0:T(8,128)(2,1)S(1)} %get-tuple-element.11), channel_id=1, source_target_pairs={{8,0},{16,8},{24,16},{9,1},{17,9},{25,17},{10,2},{18,10},{26,18},{... | collective-permute-start | bytes 393224 | tf_op jit(solution)/shard_map/ppermute | solution.py:21
  148.8 3.6 %copy-start.11 = (s32[1024]{0:T(1024)S(1)}, s32[1024]{0:T(1024)}, u32[]{:S(2)}) copy-start(s32[1024]{0:T(1024)} %pad_clamp_fusion.1) | copy-start | bytes 12292
  152.4 2.6 %copy-start.14 = (pred[8,8]{1,0:T(8,128)(4,1)S(1)}, pred[8,8]{1,0:T(8,128)(4,1)}, u32[]{:S(2)}) copy-start(pred[8,8]{1,0:T(8,128)(4,1)} %compare_and_fusion) | copy-start | bytes 196
  168.0 2.4 %copy-start = (bf16[512,128]{1,0:T(8,128)(2,1)S(1)}, bf16[512,128]{1,0:T(8,128)(2,1)}, u32[]{:S(2)}) copy-start(bf16[512,128]{1,0:T(8,128)(2,1)} %fusion.29) | copy-start | bytes 393220
Sparse Core Ops, SparseCore 0:
  8.9 26.6 all-gather.4
  93.7 21.9 all-gather.6
where the time goes:
time: 179 us; the launch traced here: 178 us
  blocking collectives  75.3 us (42%)
  local copies, waits for them, and re-layouts  43.4 us (24%)
  matrix products  19.4 us (11%)
  between operations  13.8 us (8%)
  waiting for transfers between devices  9.68 us (5%)
  other arithmetic  8.83 us (5%)
  starting transfers between devices  7.59 us (4%)
    all_gather x2, blocking collectives, layer(): lax.all_gather(gain, 'tp', axis=0, tiled=True)  22.2 us
    all_gather x2, blocking collectives, layer(): lax.all_gather(w_value, 'sp', axis=0, tiled=True)  18.8 us
    all_gather x2, blocking collectives, layer(): lax.all_gather(w_query, 'sp', axis=0, tiled=True)  17.9 us
    all_gather x2, blocking collectives, layer(): lax.all_gather(w_key, 'sp', axis=0, tiled=True)  16.5 us
    gather x6, local copies, waits for them, and re-layouts, one_row(): key_block = lax.dynamic_slice_in_dim(keys, local, 8, 0)[:, key_cols]  12.4 us
    gather x6, local copies, waits for them, and re-layouts, one_row(): value_block = lax.dynamic_slice_in_dim(values, local, 8, 0)[:, key_cols]  12.3 us
    gather x4, local copies, waits for them, and re-layouts, attend(): column_bias = table[:, :, column_offset]  12.1 us
    dot_general x2, matrix products, one_row(): jnp.einsum('jqhe,mjkhe->hjqmk', query_row, key_block, preferred_element_t...  9.08 us
  transfers between devices with their start and end apart: 6, of which 4 were waited for; matrix products, arithmetic and copies ran while one was open for 10% of the time, Pallas kernels for 0%

commit v1 on v0

v1 whole, which is shorter than its diff:
```python
import functools

import jax
import jax.numpy as jnp
from jax import lax
from jax.experimental import pallas as pl
from jax.experimental.pallas import tpu as pltpu
from jax.sharding import PartitionSpec as P

GRID_W = 64
WIN_R = 8
WIN_C = 16
HALO = 4
GAIN_ROWS = 16
epsilon = 1e-06
MESH = pl.DeviceIdType.MESH


def build_bias(table_ref, rows_ref, tiles_ref):
    rows_ref[...] = jnp.zeros_like(rows_ref)
    rows_ref[0 : 2 * WIN_R - 1, 0 : 2 * WIN_C - 1] = table_ref[0]
    shape = (GRID_W, 2 * GRID_W)
    column = lax.broadcasted_iota(jnp.int32, shape, 0)
    key_column = lax.broadcasted_iota(jnp.int32, shape, 1)
    key_column = jnp.where(key_column >= GRID_W, key_column - GRID_W, key_column)
    start = jnp.clip(column - WIN_C // 2, 0, GRID_W - WIN_C)
    inside = (key_column >= start) & (key_column < start + WIN_C)
    for o in range(2 * WIN_R - 2):
        pair = rows_ref[o : o + 1, :] + pltpu.roll(rows_ref[o + 1 : o + 2, :], GRID_W, 1)
        tile = pltpu.roll(
            jnp.broadcast_to(pair, shape), 2 * GRID_W - (WIN_C - 1), 1, stride=1, stride_axis=0
        )
        tiles_ref[o] = jnp.where(inside, tile, -1e30)


def kernel(
    n_sp,
    n_tp,
    x_ref,
    gains_ref,
    wq_a,
    wk_a,
    wv_a,
    wq_b,
    wk_b,
    wv_b,
    table_a,
    table_b,
    out_ref,
    xg_a,
    xg_b,
    wkv_a,
    wkv_b,
    wqg_a,
    wqg_b,
    kvp_a,
    kvp_b,
    q_buf,
    normed,
    rows_buf,
    tiles_a,
    tiles_b,
    load_sem,
    xs_sem,
    xr_sem,
    ws_sem,
    wr_sem,
    hs_sem,
    hr_sem,
):
    sp = lax.axis_index("sp")
    tp = lax.axis_index("tp")
    tokens, feat = x_ref.shape
    depth = wq_a.shape[0]
    rows_dev = tokens // GRID_W
    total_rows = rows_dev * n_sp
    half = n_tp // 2
    core = lax.rem(tp, 2)
    partner = tp + 1 - 2 * core
    low = HALO * GRID_W
    below = (HALO - 1 if rows_dev >= WIN_R else HALO) * GRID_W
    factor = feat ** (-0.5)

    xg = (xg_a, xg_b)
    wkv = (wkv_a, wkv_b)
    wqg = (wqg_a, wqg_b)
    kvp = (kvp_a, kvp_b)
    tiles = (tiles_a, tiles_b)

    def w_rows(device):
        return pl.ds(pl.multiple_of(device * depth, depth), depth)

    mine = w_rows(sp)
    loads = [
        (x_ref, xg_a.at[tp, pl.ds(0, tokens)]),
        (gains_ref, xg_a.at[tp, pl.ds(tokens, GAIN_ROWS)]),
        (wk_a, wkv_a.at[mine, pl.ds(0, feat)]),
        (wv_a, wkv_a.at[mine, pl.ds(feat, feat)]),
        (wq_a, wqg_a.at[mine]),
        (wk_b, wkv_b.at[mine, pl.ds(0, feat)]),
        (wv_b, wkv_b.at[mine, pl.ds(feat, feat)]),
        (wq_b, wqg_b.at[mine]),
    ]
    loads = [pltpu.make_async_copy(s, d, load_sem.at[i]) for i, (s, d) in enumerate(loads)]
    for load in loads:
        load.start()

    barrier = pltpu.get_barrier_semaphore()
    chip_peers = [lax.rem(tp + 2 * k, n_tp) for k in range(1, half)]
    chip_sources = [lax.rem(tp + n_tp - 2 * k, n_tp) for k in range(1, half)]
    sp_peers = [lax.rem(sp + k, n_sp) for k in range(1, n_sp)]
    sp_sources = [lax.rem(sp + n_sp - k, n_sp) for k in range(1, n_sp)]
    for t in [partner] + chip_peers:
        pl.semaphore_signal(barrier, inc=1, device_id=(sp, t), device_id_type=MESH)
    for s in sp_peers:
        pl.semaphore_signal(barrier, inc=1, device_id=(s, tp), device_id_type=MESH)
    pl.semaphore_wait(barrier, half + n_sp - 1)

    def remote(src, dst, send, recv, device):
        return pltpu.make_async_remote_copy(
            src_ref=src,
            dst_ref=dst,
            send_sem=send,
            recv_sem=recv,
            device_id=device,
            device_id_type=MESH,
        )

    sent = []

    def x_slot(layer, slot):
        if layer == 0:
            return xg[0].at[slot]
        return xg[1].at[slot]

    def x_copy(layer, slot, index, target):
        ref = x_slot(layer, slot)
        return remote(ref, ref, xs_sem.at[layer, index], xr_sem.at[layer, slot], (sp, target))

    def x_start(layer):
        for index, target in enumerate(chip_peers + [partner]):
            copy = x_copy(layer, tp, index, target)
            copy.start()
            sent.append(copy)

    def x_finish(layer):
        for index, slot in enumerate(chip_sources):
            x_copy(layer, slot, half + index, partner).wait_recv()
            copy = x_copy(layer, slot, half + index, partner)
            copy.start()
            sent.append(copy)
        for k in range(half):
            slot = lax.rem(partner + n_tp - 2 * k, n_tp)
            x_copy(layer, slot, 0, partner).wait_recv()

    def w_copy(layer, which, slot, index, target):
        ref = (wkv, wqg)[which][layer].at[w_rows(slot)]
        return remote(
            ref, ref, ws_sem.at[layer, which, index], wr_sem.at[layer, which, slot], (target, tp)
        )

    def w_start(layer, which):
        for index, target in enumerate(sp_peers):
            copy = w_copy(layer, which, sp, index, target)
            copy.start()
            sent.append(copy)

    def w_finish(layer, which):
        for slot in sp_sources:
            w_copy(layer, which, slot, 0, slot).wait_recv()

    def down(layer):
        buf = kvp[layer]
        return remote(
            buf.at[pl.ds(tokens, low)],
            buf.at[pl.ds(0, low)],
            hs_sem.at[layer, 0],
            hr_sem.at[layer, 0],
            (lax.rem(sp + 1, n_sp), tp),
        )

    def up(layer):
        buf = kvp[layer]
        return remote(
            buf.at[pl.ds(low, below)],
            buf.at[pl.ds(low + tokens, below)],
            hs_sem.at[layer, 1],
            hr_sem.at[layer, 1],
            (lax.rem(sp + n_sp - 1, n_sp), tp),
        )

    has_next = sp < n_sp - 1
    has_previous = sp > 0

    def norm(layer):
        chunk = GRID_W
        buf = xg[layer]
        for c in range(tokens // chunk):
            at = pl.ds(c * chunk, chunk)
            total = jnp.zeros((chunk, feat), jnp.float32)
            for s in range(n_tp):
                wide = buf[s, at, :].astype(jnp.float32)
                total = total + wide * wide
            mean = jnp.sum(total, axis=-1, keepdims=True) * (1.0 / (n_tp * feat))
            scale = lax.rsqrt(mean + epsilon)
            for s in range(n_tp):
                gain = xg_a[s, pl.ds(tokens, GAIN_ROWS), :][layer : layer + 1, :]
                wide = buf[s, at, :].astype(jnp.float32)
                normed[at, s * feat : (s + 1) * feat] = (
                    wide * scale * gain.astype(jnp.float32)
                ).astype(jnp.bfloat16)

    def project(weights, dst, offset):
        chunk = 2 * GRID_W if tokens % (2 * GRID_W) == 0 else GRID_W
        for c in range(tokens // chunk):
            made = jnp.dot(
                normed[c * chunk : (c + 1) * chunk, :],
                weights[...],
                preferred_element_type=jnp.float32,
            )
            dst[pl.ds(offset + c * chunk, chunk), :] = made.astype(jnp.bfloat16)

    def attend(layer, index):
        row = sp * rows_dev + index
        first = jnp.minimum(jnp.maximum(row - HALO, 0), total_rows - WIN_R)
        local = first - sp * rows_dev + HALO
        base = first - row + WIN_R - 1
        at = pl.ds(pl.multiple_of(local * GRID_W, GRID_W), WIN_R * GRID_W)
        keys = kvp[layer][at, 0:feat]
        values = kvp[layer][at, feat : 2 * feat]
        query = q_buf[index * GRID_W : (index + 1) * GRID_W, :]
        scores = lax.dot_general(
            query, keys, (((1,), (1,)), ((), ())), preferred_element_type=jnp.float32
        )
        bias = jnp.concatenate([tiles[layer][base + 2 * j] for j in range(WIN_R // 2)], axis=1)
        scores = scores * factor + bias
        top = jnp.max(scores, axis=-1, keepdims=True)
        weight = jnp.exp(scores - top)
        weight = weight * (1.0 / jnp.sum(weight, axis=-1, keepdims=True))
        out = jnp.dot(weight.astype(jnp.bfloat16), values, preferred_element_type=jnp.float32)
        here = pl.ds(index * GRID_W, GRID_W)
        wide = xg[layer][tp, here, :].astype(jnp.float32)
        return (wide + out).astype(jnp.bfloat16)

    loads[0].wait()
    loads[1].wait()
    x_start(0)
    loads[2].wait()
    loads[3].wait()
    w_start(0, 0)
    loads[4].wait()
    w_start(0, 1)
    build_bias(table_a, rows_buf, tiles_a)
    build_bias(table_b, rows_buf, tiles_b)
    for load in loads[5:]:
        load.wait()

    for layer in range(2):
        x_finish(layer)
        norm(layer)
        w_finish(layer, 0)
        project(wkv[layer], kvp[layer], low)

        @pl.when(has_next)
        def _():
            down(layer).start()

        @pl.when(has_previous)
        def _():
            up(layer).start()

        if layer == 0:
            w_start(1, 0)
            w_start(1, 1)
        w_finish(layer, 1)
        project(wqg[layer], q_buf, 0)

        @pl.when(has_previous)
        def _():
            down(layer).wait_recv()

        @pl.when(has_next)
        def _():
            up(layer).wait_recv()

        for index in range(rows_dev):
            made = attend(layer, index)
            here = pl.ds(index * GRID_W, GRID_W)
            if layer == 0:
                xg_b[tp, here, :] = made
            else:
                out_ref[here, :] = made
        if layer == 0:
            x_start(1)

    for layer in range(2):

        @pl.when(has_next)
        def _():
            down(layer).wait_send()

        @pl.when(has_previous)
        def _():
            up(layer).wait_send()

    for copy in sent:
        copy.wait_send()


def body(n_sp, n_tp, stream, gain_a, wq_a, wk_a, wv_a, table_a, gain_b, wq_b, wk_b, wv_b, table_b):
    tokens, feat = stream.shape
    depth = wq_a.shape[0] * n_sp
    gains = jnp.pad(jnp.stack([gain_a, gain_b]), ((0, GAIN_ROWS - 2), (0, 0)))
    bf16 = jnp.bfloat16
    padded = tokens + 2 * HALO * GRID_W
    hbm = pl.BlockSpec(memory_space=pl.ANY)
    vmem = pl.BlockSpec(memory_space=pltpu.VMEM)
    dma = pltpu.SemaphoreType.DMA
    return pl.pallas_call(
        functools.partial(kernel, n_sp, n_tp),
        out_shape=jax.ShapeDtypeStruct((tokens, feat), bf16),
        in_specs=[hbm] * 8 + [vmem] * 2,
        out_specs=vmem,
        scratch_shapes=[
            pltpu.VMEM((n_tp, tokens + GAIN_ROWS, feat), bf16),
            pltpu.VMEM((n_tp, tokens, feat), bf16),
            pltpu.VMEM((depth, 2 * feat), bf16),
            pltpu.VMEM((depth, 2 * feat), bf16),
            pltpu.VMEM((depth, feat), bf16),
            pltpu.VMEM((depth, feat), bf16),
            pltpu.VMEM((padded, 2 * feat), bf16),
            pltpu.VMEM((padded, 2 * feat), bf16),
            pltpu.VMEM((tokens, feat), bf16),
            pltpu.VMEM((tokens, n_tp * feat), bf16),
            pltpu.VMEM((2 * WIN_R, 2 * GRID_W), jnp.float32),
            pltpu.VMEM((2 * WIN_R - 2, GRID_W, 2 * GRID_W), jnp.float32),
            pltpu.VMEM((2 * WIN_R - 2, GRID_W, 2 * GRID_W), jnp.float32),
            dma((8,)),
            dma((2, n_tp)),
            dma((2, n_tp)),
            dma((2, 2, n_sp)),
            dma((2, 2, n_sp)),
            dma((2, 2)),
            dma((2, 2)),
        ],
        compiler_params=pltpu.CompilerParams(collective_id=0, has_side_effects=True),
    )(stream, gains, wq_a, wk_a, wv_a, wq_b, wk_b, wv_b, table_a, table_b)


def solution(mesh):
    placed = (
        P("sp", "tp"),
        P("tp"),
        P("sp", "tp"),
        P("sp", "tp"),
        P("sp", "tp"),
        P("tp", None, None),
        P("tp"),
        P("sp", "tp"),
        P("sp", "tp"),
        P("sp", "tp"),
        P("tp", None, None),
    )
    return jax.shard_map(
        functools.partial(body, mesh.shape["sp"], mesh.shape["tp"]),
        mesh=mesh,
        in_specs=placed,
        out_specs=P("sp", "tp"),
        check_vma=False,
    )
```

time: 179 us -> 58.1 us (0.32)
  the two profiles are of different devices: /device:TPU:0 before, /device:TPU:24 now
where the time goes in v1:
time: 58.1 us; the launch traced here: 57.8 us
  Pallas kernels  53.6 us (92%)
  local copies, waits for them, and re-layouts  2.87 us (5%)
  other arithmetic  1.28 us (2%)
    pallas_call x1, Pallas kernels, body(): pl.pallas_call(functools.partial(kernel, n_sp, n_tp), out_shape=jax.Shape...  53.6 us
    unnamed x7, local copies, waits for them, and re-layouts  2.87 us
    another operation x1, other arithmetic, body(): gains = jnp.pad(jnp.stack([gain_a, gain_b]), ((0, GAIN_ROWS - 2), (0, 0)))  1.28 us

profile of v1, /device:TPU:24, one launch (start us, length us, event | category | flops | bytes accessed | tf_op | source)
XLA Modules:
  0.0 57.8 jit_solution(7736588275457170039)
XLA Ops:
  0.0 0.0 copy-start
  0.0 1.3 %fusion.2.gains_ref = bf16[16,128]{1,0:T(8,128)(2,1)} fusion(bf16[1,128]{1,0:T(2,128)(2,1)} %bitcast.2, bf16[1,128]{1,0:T(2,128)(2,1)} %bitcast.3), kind=kLoop, calls=%fused_computation.3 | loop fusion | flops 14336 | bytes 4608 | tf_op jit(solution)/shard_map/stack | solution.py:313
  1.3 0.0 copy-done
  1.3 0.0 copy-start.1
  1.3 0.6 %copy.12.table_a = f32[1,15,31]{2,1,0:T(8,128)} copy(f32[1,15,31]{2,0,1:T(1,128)S(1)} %copy-done) | data formatting | bytes 3720 | tf_op args[5]
  1.9 0.1 copy-done.1
  2.0 0.6 %copy.13.table_b = f32[1,15,31]{2,1,0:T(8,128)} copy(f32[1,15,31]{2,0,1:T(1,128)S(1)} %copy-done.1) | data formatting | bytes 3720 | tf_op args[10]
  2.6 53.6 %shard_map.109 = bf16[512,128]{1,0:T(8,128)(2,1)} custom-call(bf16[512,128]{1,0:T(8,128)(2,1)} %x_ref.1, bf16[16,128]{1,0:T(8,128)(2,1)} %fusion.2.gains_ref, bf16[256,128]{1,0:T(8,128)(2,1)} %wq_a.1, bf16[256,128]{1,0:T(8,128)(2,1)} %wk_a.1, bf16[256,128]{1,0:T(8,128)(2,1)} %wv_a.1, bf16[256,128]{1,0:T(8,128)(2,1)} %wq_b.1, bf16[256,128]{1,0:T(8,128)(2,1)} %wk_b.1, ...), custom_call_target="tpu_custom_call" | custom-call | tf_op jit(solution)/shard_map/pallas_call | solution.py:319
  56.2 1.6 %copy.15 = bf16[512,128]{1,0:T(8,128)(2,1)} copy(bf16[512,128]{1,0:T(8,128)(2,1)} %shard_map.109) | data formatting | bytes 262144
Async XLA Ops:
  0.0 1.3 %copy-start = (f32[1,15,31]{2,0,1:T(1,128)S(1)}, f32[1,15,31]{2,0,1:T(1,128)}, u32[]{:S(2)}) copy-start(f32[1,15,31]{2,0,1:T(1,128)} %param.16) | copy-start | bytes 5584
  1.3 0.7 %copy-start.1 = (f32[1,15,31]{2,0,1:T(1,128)S(1)}, f32[1,15,31]{2,0,1:T(1,128)}, u32[]{:S(2)}) copy-start(f32[1,15,31]{2,0,1:T(1,128)} %param.21) | copy-start | bytes 5584

commit v2 on v1

--- a/solution.py
+++ b/solution.py
@@ -18,7 +18,7 @@
 
 def build_bias(table_ref, rows_ref, tiles_ref):
     rows_ref[...] = jnp.zeros_like(rows_ref)
-    rows_ref[0 : 2 * WIN_R - 1, 0 : 2 * WIN_C - 1] = table_ref[0]
+    rows_ref[0 : 2 * WIN_R - 1, 0 : 2 * WIN_C - 1] = table_ref[:, 0, :]
     shape = (GRID_W, 2 * GRID_W)
     column = lax.broadcasted_iota(jnp.int32, shape, 0)
     key_column = lax.broadcasted_iota(jnp.int32, shape, 1)
@@ -37,7 +37,8 @@
     n_sp,
     n_tp,
     x_ref,
-    gains_ref,
+    gain_a,
+    gain_b,
     wq_a,
     wk_a,
     wv_a,
@@ -62,6 +63,8 @@
     tiles_b,
     load_sem,
     xs_sem,
+    xf_sem,
+    xl_sem,
     xr_sem,
     ws_sem,
     wr_sem,
@@ -76,6 +79,12 @@
     total_rows = rows_dev * n_sp
     half = n_tp // 2
     core = lax.rem(tp, 2)
+    z = tp // 2
+    group = 2 if rows_dev % 2 == 0 else 1
+    chunk = group * GRID_W
+    count = rows_dev // group
+    low_half = tuple(range(count // 2, count)) + tuple(range(count // 2))
+    orders = (low_half, tuple(range(count)))
     partner = tp + 1 - 2 * core
     low = HALO * GRID_W
     below = (HALO - 1 if rows_dev >= WIN_R else HALO) * GRID_W
@@ -91,9 +100,15 @@
         return pl.ds(pl.multiple_of(device * depth, depth), depth)
 
     mine = w_rows(sp)
+    def place(layer, part):
+        if layer == 1:
+            return part * chunk
+        return GAIN_ROWS + orders[0].index(part) * chunk
+
     loads = [
-        (x_ref, xg_a.at[tp, pl.ds(0, tokens)]),
-        (gains_ref, xg_a.at[tp, pl.ds(tokens, GAIN_ROWS)]),
+        (x_ref.at[pl.ds(part * chunk, chunk)], xg_a.at[tp, pl.ds(place(0, part), chunk)])
+        for part in orders[0]
+    ] + [
         (wk_a, wkv_a.at[mine, pl.ds(0, feat)]),
         (wv_a, wkv_a.at[mine, pl.ds(feat, feat)]),
         (wq_a, wqg_a.at[mine]),
@@ -104,10 +119,12 @@
     loads = [pltpu.make_async_copy(s, d, load_sem.at[i]) for i, (s, d) in enumerate(loads)]
     for load in loads:
         load.start()
+    spare = jnp.zeros((GAIN_ROWS - 2, feat), jnp.float32)
+    both = [gain_a[...].astype(jnp.float32), gain_b[...].astype(jnp.float32), spare]
+    xg_a[tp, 0:GAIN_ROWS, :] = jnp.concatenate(both, axis=0).astype(jnp.bfloat16)
 
     barrier = pltpu.get_barrier_semaphore()
     chip_peers = [lax.rem(tp + 2 * k, n_tp) for k in range(1, half)]
-    chip_sources = [lax.rem(tp + n_tp - 2 * k, n_tp) for k in range(1, half)]
     sp_peers = [lax.rem(sp + k, n_sp) for k in range(1, n_sp)]
     sp_sources = [lax.rem(sp + n_sp - k, n_sp) for k in range(1, n_sp)]
     for t in [partner] + chip_peers:
@@ -128,30 +145,46 @@
 
     sent = []
 
-    def x_slot(layer, slot):
-        if layer == 0:
-            return xg[0].at[slot]
-        return xg[1].at[slot]
-
-    def x_copy(layer, slot, index, target):
-        ref = x_slot(layer, slot)
-        return remote(ref, ref, xs_sem.at[layer, index], xr_sem.at[layer, slot], (sp, target))
-
-    def x_start(layer):
-        for index, target in enumerate(chip_peers + [partner]):
-            copy = x_copy(layer, tp, index, target)
+    def x_copy(layer, part, slot, sem, target):
+        at, size = place(layer, part), chunk
+        if layer == 0 and part == orders[0][0]:
+            at, size = 0, chunk + GAIN_ROWS
+        ref = xg[layer].at[slot, pl.ds(at, size)]
+        return remote(ref, ref, sem, xr_sem.at[layer, part, slot], (sp, target))
+
+    def begin(copy, condition=None):
+        sent.append((copy, condition))
+        if condition is None:
             copy.start()
-            sent.append(copy)
-
-    def x_finish(layer):
-        for index, slot in enumerate(chip_sources):
-            x_copy(layer, slot, half + index, partner).wait_recv()
-            copy = x_copy(layer, slot, half + index, partner)
-            copy.start()
-            sent.append(copy)
+        else:
+            pl.when(condition)(copy.start)
+
+    def x_start(layer, part):
+        begin(x_copy(layer, part, tp, xf_sem.at[layer, part, tp], partner))
+        for k in range(half - 1, 0, -1):
+            right = z + k <= half - 2
+            left = z - k >= 1
+            if k == 1:
+                right = right | (z == half - 2)
+                left = left | (z == 1)
+            sem = xs_sem.at[layer, part, k]
+            begin(x_copy(layer, part, tp, sem, tp + 2 * k), right)
+            sem = xs_sem.at[layer, part, half + k]
+            begin(x_copy(layer, part, tp, sem, tp - 2 * k), left)
+
+    def x_finish(layer, part):
+        for k in range(1, half):
+            slot = lax.rem(tp + 2 * k, n_tp)
+            relay = xl_sem.at[layer, part, slot]
+            x_copy(layer, part, slot, relay, partner).wait_recv()
+            right = x_copy(layer, part, slot, relay, tp + 2)
+            begin(right, (slot < tp) & (z == half - 2))
+            left = x_copy(layer, part, slot, relay, tp - 2)
+            begin(left, (slot > tp) & (z == 1))
+            begin(x_copy(layer, part, slot, xf_sem.at[layer, part, slot], partner))
         for k in range(half):
-            slot = lax.rem(partner + n_tp - 2 * k, n_tp)
-            x_copy(layer, slot, 0, partner).wait_recv()
+            slot = lax.rem(partner + 2 * k, n_tp)
+            x_copy(layer, part, slot, xf_sem.at[layer, part, slot], partner).wait_recv()
 
     def w_copy(layer, which, slot, index, target):
         ref = (wkv, wqg)[which][layer].at[w_rows(slot)]
@@ -161,9 +194,7 @@
 
     def w_start(layer, which):
         for index, target in enumerate(sp_peers):
-            copy = w_copy(layer, which, sp, index, target)
-            copy.start()
-            sent.append(copy)
+            begin(w_copy(layer, which, sp, index, target))
 
     def w_finish(layer, which):
         for slot in sp_sources:
@@ -192,33 +223,31 @@
     has_next = sp < n_sp - 1
     has_previous = sp > 0
 
-    def norm(layer):
-        chunk = GRID_W
+    def norm(layer, part):
         buf = xg[layer]
-        for c in range(tokens // chunk):
-            at = pl.ds(c * chunk, chunk)
-            total = jnp.zeros((chunk, feat), jnp.float32)
+        for c in range(group):
+            at = pl.ds(place(layer, part) + c * GRID_W, GRID_W)
+            to = pl.ds(part * chunk + c * GRID_W, GRID_W)
+            total = jnp.zeros((GRID_W, feat), jnp.float32)
             for s in range(n_tp):
                 wide = buf[s, at, :].astype(jnp.float32)
                 total = total + wide * wide
             mean = jnp.sum(total, axis=-1, keepdims=True) * (1.0 / (n_tp * feat))
             scale = lax.rsqrt(mean + epsilon)
             for s in range(n_tp):
-                gain = xg_a[s, pl.ds(tokens, GAIN_ROWS), :][layer : layer + 1, :]
+                gain = xg_a[s, 0:GAIN_ROWS, :][layer : layer + 1, :]
                 wide = buf[s, at, :].astype(jnp.float32)
-                normed[at, s * feat : (s + 1) * feat] = (
+                normed[to, s * feat : (s + 1) * feat] = (
                     wide * scale * gain.astype(jnp.float32)
                 ).astype(jnp.bfloat16)
 
-    def project(weights, dst, offset):
-        chunk = 2 * GRID_W if tokens % (2 * GRID_W) == 0 else GRID_W
-        for c in range(tokens // chunk):
-            made = jnp.dot(
-                normed[c * chunk : (c + 1) * chunk, :],
-                weights[...],
-                preferred_element_type=jnp.float32,
-            )
-            dst[pl.ds(offset + c * chunk, chunk), :] = made.astype(jnp.bfloat16)
+    def project(weights, dst, offset, part):
+        made = jnp.dot(
+            normed[part * chunk : (part + 1) * chunk, :],
+            weights[...],
+            preferred_element_type=jnp.float32,
+        )
+        dst[pl.ds(offset + part * chunk, chunk), :] = made.astype(jnp.bfloat16)
 
     def attend(layer, index):
         row = sp * rows_dev + index
@@ -238,79 +267,87 @@
         weight = jnp.exp(scores - top)
         weight = weight * (1.0 / jnp.sum(weight, axis=-1, keepdims=True))
         out = jnp.dot(weight.astype(jnp.bfloat16), values, preferred_element_type=jnp.float32)
-        here = pl.ds(index * GRID_W, GRID_W)
-        wide = xg[layer][tp, here, :].astype(jnp.float32)
+        start = place(layer, index // group) + index % group * GRID_W
+        wide = xg[layer][tp, pl.ds(start, GRID_W), :].astype(jnp.float32)
         return (wide + out).astype(jnp.bfloat16)
 
-    loads[0].wait()
-    loads[1].wait()
-    x_start(0)
-    loads[2].wait()
-    loads[3].wait()
+    for load, part in zip(loads, orders[0]):
+        load.wait()
+        x_start(0, part)
+    rest = loads[count:]
+    rest[0].wait()
+    rest[1].wait()
     w_start(0, 0)
-    loads[4].wait()
+    rest[2].wait()
     w_start(0, 1)
     build_bias(table_a, rows_buf, tiles_a)
     build_bias(table_b, rows_buf, tiles_b)
-    for load in loads[5:]:
+    for load in rest[3:]:
         load.wait()
 
+    top_rows = [i for i in range(rows_dev) if i < HALO]
+    end_rows = [i for i in range(rows_dev) if i + HALO > rows_dev]
+    up_parts = {i // group for i in range(below // GRID_W)}
+    down_parts = {i // group for i in range(rows_dev - HALO, rows_dev)}
+
     for layer in range(2):
-        x_finish(layer)
-        norm(layer)
-        w_finish(layer, 0)
-        project(wkv[layer], kvp[layer], low)
-
-        @pl.when(has_next)
-        def _():
-            down(layer).start()
-
-        @pl.when(has_previous)
-        def _():
-            up(layer).start()
-
+        done = set()
+        for part in orders[layer]:
+            x_finish(layer, part)
+            norm(layer, part)
+            if not done:
+                w_finish(layer, 0)
+            project(wkv[layer], kvp[layer], low, part)
+            before = set(done)
+            done.add(part)
+            if down_parts <= done and not down_parts <= before:
+                pl.when(has_next)(down(layer).start)
+            if up_parts <= done and not up_parts <= before:
+                pl.when(has_previous)(up(layer).start)
         if layer == 0:
             w_start(1, 0)
             w_start(1, 1)
         w_finish(layer, 1)
-        project(wqg[layer], q_buf, 0)
-
-        @pl.when(has_previous)
-        def _():
-            down(layer).wait_recv()
-
-        @pl.when(has_next)
-        def _():
-            up(layer).wait_recv()
-
-        for index in range(rows_dev):
-            made = attend(layer, index)
-            here = pl.ds(index * GRID_W, GRID_W)
-            if layer == 0:
+        for part in orders[layer]:
+            project(wqg[layer], q_buf, 0, part)
+
+        late = end_rows if layer == 0 else top_rows
+        early = top_rows if layer == 0 else end_rows
+        early = [i for i in early if i not in late]
+        inner = [i for i in range(rows_dev) if i not in late and i not in early]
+        finished = set()
+        for rows, wait in ((inner, None), (early, layer == 0), (late, layer == 1)):
+            if wait is True:
+                pl.when(has_previous)(down(layer).wait_recv)
+            if wait is False:
+                pl.when(has_next)(up(layer).wait_recv)
+            for index in rows:
+                made = attend(layer, index)
+                here = pl.ds(index * GRID_W, GRID_W)
+                if layer == 1:
+                    out_ref[here, :] = made
+                    continue
                 xg_b[tp, here, :] = made
-            else:
-                out_ref[here, :] = made
-        if layer == 0:
-            x_start(1)
+                finished.add(index)
+                part = index // group
+                if all(part * group + i in finished for i in range(group)):
+                    x_start(1, part)
 
     for layer in range(2):
-
-        @pl.when(has_next)
-        def _():
-            down(layer).wait_send()
-
-        @pl.when(has_previous)
-        def _():
-            up(layer).wait_send()
-
-    for copy in sent:
-        copy.wait_send()
+        pl.when(has_next)(down(layer).wait_send)
+        pl.when(has_previous)(up(layer).wait_send)
+    for copy, condition in sent:
+        if condition is None:
+            copy.wait_send()
+        else:
+            pl.when(condition)(copy.wait_send)
 
 
 def body(n_sp, n_tp, stream, gain_a, wq_a, wk_a, wv_a, table_a, gain_b, wq_b, wk_b, wv_b, table_b):
     tokens, feat = stream.shape
     depth = wq_a.shape[0] * n_sp
-    gains = jnp.pad(jnp.stack([gain_a, gain_b]), ((0, GAIN_ROWS - 2), (0, 0)))
+    rows_dev = tokens // GRID_W
+    parts = rows_dev // 2 if rows_dev % 2 == 0 else rows_dev
     bf16 = jnp.bfloat16
     padded = tokens + 2 * HALO * GRID_W
     hbm = pl.BlockSpec(memory_space=pl.ANY)
@@ -319,7 +356,7 @@
     return pl.pallas_call(
         functools.partial(kernel, n_sp, n_tp),
         out_shape=jax.ShapeDtypeStruct((tokens, feat), bf16),
-        in_specs=[hbm] * 8 + [vmem] * 2,
+        in_specs=[hbm] + [vmem] * 2 + [hbm] * 6 + [vmem] * 2,
         out_specs=vmem,
         scratch_shapes=[
             pltpu.VMEM((n_tp, tokens + GAIN_ROWS, feat), bf16),
@@ -335,16 +372,30 @@
             pltpu.VMEM((2 * WIN_R, 2 * GRID_W), jnp.float32),
             pltpu.VMEM((2 * WIN_R - 2, GRID_W, 2 * GRID_W), jnp.float32),
             pltpu.VMEM((2 * WIN_R - 2, GRID_W, 2 * GRID_W), jnp.float32),
-            dma((8,)),
-            dma((2, n_tp)),
-            dma((2, n_tp)),
+            dma((parts + 6,)),
+            dma((2, parts, n_tp)),
+            dma((2, parts, n_tp)),
+            dma((2, parts, n_tp)),
+            dma((2, parts, n_tp)),
             dma((2, 2, n_sp)),
             dma((2, 2, n_sp)),
             dma((2, 2)),
             dma((2, 2)),
         ],
         compiler_params=pltpu.CompilerParams(collective_id=0, has_side_effects=True),
-    )(stream, gains, wq_a, wk_a, wv_a, wq_b, wk_b, wv_b, table_a, table_b)
+    )(
+        stream,
+        gain_a.reshape(1, feat),
+        gain_b.reshape(1, feat),
+        wq_a,
+        wk_a,
+        wv_a,
+        wq_b,
+        wk_b,
+        wv_b,
+        jnp.transpose(table_a, (1, 0, 2)),
+        jnp.transpose(table_b, (1, 0, 2)),
+    )
 
 
 def solution(mesh):

time: 58.1 us -> 47.7 us (0.82)
  the two profiles are of different devices: /device:TPU:24 before, /device:TPU:5 now
where the time goes in v2:
time: 47.7 us; the launch traced here: 47.5 us
  Pallas kernels  45.9 us (96%)
  local copies, waits for them, and re-layouts  1.57 us (3%)
    pallas_call x1, Pallas kernels, body(): pl.pallas_call(functools.partial(kernel, n_sp, n_tp), out_shape=jax.Shape...  45.9 us
    unnamed x1, local copies, waits for them, and re-layouts  1.57 us

profile of v2, /device:TPU:5, one launch (start us, length us, event | category | flops | bytes accessed | tf_op | source)
XLA Modules:
  0.0 47.5 jit_solution(5401637319444257387)
XLA Ops:
  0.0 45.9 %shard_map.109 = bf16[512,128]{1,0:T(8,128)(2,1)} custom-call(bf16[512,128]{1,0:T(8,128)(2,1)} %x_ref.1, bf16[1,128]{1,0:T(2,128)(2,1)} %bitcast.6, bf16[1,128]{1,0:T(2,128)(2,1)} %bitcast.7, bf16[256,128]{1,0:T(8,128)(2,1)} %wq_a.1, bf16[256,128]{1,0:T(8,128)(2,1)} %wk_a.1, bf16[256,128]{1,0:T(8,128)(2,1)} %wv_a.1, bf16[256,128]{1,0:T(8,128)(2,1)} %wq_b.1, ...), custom_call_target="tpu_custom_call" | custom-call | tf_op jit(solution)/shard_map/pallas_call | solution.py:356
  45.9 1.6 %copy.13 = bf16[512,128]{1,0:T(8,128)(2,1)} copy(bf16[512,128]{1,0:T(8,128)(2,1)} %shard_map.109) | data formatting | bytes 262144

commit v3 on v2

--- a/solution.py
+++ b/solution.py
@@ -80,7 +80,7 @@
     half = n_tp // 2
     core = lax.rem(tp, 2)
     z = tp // 2
-    group = 2 if rows_dev % 2 == 0 else 1
+    group = rows_dev // 2 if rows_dev % 2 == 0 else 1
     chunk = group * GRID_W
     count = rows_dev // group
     low_half = tuple(range(count // 2, count)) + tuple(range(count // 2))
@@ -161,12 +161,9 @@
 
     def x_start(layer, part):
         begin(x_copy(layer, part, tp, xf_sem.at[layer, part, tp], partner))
-        for k in range(half - 1, 0, -1):
-            right = z + k <= half - 2
-            left = z - k >= 1
-            if k == 1:
-                right = right | (z == half - 2)
-                left = left | (z == 1)
+        for k in range(1, half):
+            right = z + k <= half - (1 if k <= 2 else 2)
+            left = z - k >= (0 if k <= 2 else 1)
             sem = xs_sem.at[layer, part, k]
             begin(x_copy(layer, part, tp, sem, tp + 2 * k), right)
             sem = xs_sem.at[layer, part, half + k]
@@ -178,9 +175,9 @@
             relay = xl_sem.at[layer, part, slot]
             x_copy(layer, part, slot, relay, partner).wait_recv()
             right = x_copy(layer, part, slot, relay, tp + 2)
-            begin(right, (slot < tp) & (z == half - 2))
+            begin(right, (slot < tp - 3) & (z == half - 2))
             left = x_copy(layer, part, slot, relay, tp - 2)
-            begin(left, (slot > tp) & (z == 1))
+            begin(left, (slot > tp + 3) & (z == 1))
             begin(x_copy(layer, part, slot, xf_sem.at[layer, part, slot], partner))
         for k in range(half):
             slot = lax.rem(partner + 2 * k, n_tp)
@@ -347,7 +344,7 @@
     tokens, feat = stream.shape
     depth = wq_a.shape[0] * n_sp
     rows_dev = tokens // GRID_W
-    parts = rows_dev // 2 if rows_dev % 2 == 0 else rows_dev
+    parts = 2 if rows_dev % 2 == 0 else rows_dev
     bf16 = jnp.bfloat16
     padded = tokens + 2 * HALO * GRID_W
     hbm = pl.BlockSpec(memory_space=pl.ANY)
@@ -355,7 +352,7 @@
     dma = pltpu.SemaphoreType.DMA
     return pl.pallas_call(
         functools.partial(kernel, n_sp, n_tp),
-        out_shape=jax.ShapeDtypeStruct((tokens, feat), bf16),
+        out_shape=pltpu.VMEM((tokens, feat), bf16),
         in_specs=[hbm] + [vmem] * 2 + [hbm] * 6 + [vmem] * 2,
         out_specs=vmem,
         scratch_shapes=[

time: 47.7 us -> 43.2 us (0.906)
  Pallas kernels: 45.9 us -> 42.3 us
  local copies, waits for them, and re-layouts: 1.57 us -> 0.66 us
    pallas_call x1, Pallas kernels: 45.9 us -> 42.3 us  [body(): pl.pallas_call(functools.partial(kernel, n_sp, n_tp), out_shape=pltpu.VME...]
    unnamed x1, local copies, waits for them, and re-layouts: 1.57 us -> 0.66 us
where the time goes in v3:
time: 43.2 us; the launch traced here: 42.9 us
  Pallas kernels  42.3 us (98%)
  local copies, waits for them, and re-layouts  0.66 us (2%)
    pallas_call x1, Pallas kernels, body(): pl.pallas_call(functools.partial(kernel, n_sp, n_tp), out_shape=pltpu.VME...  42.3 us

profile of v3, /device:TPU:5, one launch (start us, length us, event | category | flops | bytes accessed | tf_op | source)
XLA Modules:
  0.0 42.9 jit_solution(17525095710634812194)
XLA Ops:
  0.0 42.3 %shard_map.109 = bf16[512,128]{1,0:T(8,128)(2,1)S(1)} custom-call(bf16[512,128]{1,0:T(8,128)(2,1)} %x_ref.1, bf16[1,128]{1,0:T(2,128)(2,1)} %bitcast.6, bf16[1,128]{1,0:T(2,128)(2,1)} %bitcast.7, bf16[256,128]{1,0:T(8,128)(2,1)} %wq_a.1, bf16[256,128]{1,0:T(8,128)(2,1)} %wk_a.1, bf16[256,128]{1,0:T(8,128)(2,1)} %wv_a.1, bf16[256,128]{1,0:T(8,128)(2,1)} %wq_b.1, ...), custom_call_target="tpu_custom_call" | custom-call | tf_op jit(solution)/shard_map/pallas_call | solution.py:353
  42.3 0.7 %copy.13 = bf16[512,128]{1,0:T(8,128)(2,1)} copy(bf16[512,128]{1,0:T(8,128)(2,1)S(1)} %shard_map.109) | data formatting | bytes 262144

commit v4 on v3

--- a/solution.py
+++ b/solution.py
@@ -11,6 +11,7 @@
 WIN_R = 8
 WIN_C = 16
 HALO = 4
+BATCH = 4
 GAIN_ROWS = 16
 epsilon = 1e-06
 MESH = pl.DeviceIdType.MESH
@@ -127,11 +128,22 @@
     chip_peers = [lax.rem(tp + 2 * k, n_tp) for k in range(1, half)]
     sp_peers = [lax.rem(sp + k, n_sp) for k in range(1, n_sp)]
     sp_sources = [lax.rem(sp + n_sp - k, n_sp) for k in range(1, n_sp)]
-    for t in [partner] + chip_peers:
-        pl.semaphore_signal(barrier, inc=1, device_id=(sp, t), device_id_type=MESH)
+    ends = int(half >= 4)
+    at_end = (z == 0) | (z == half - 1)
+    pl.semaphore_signal(barrier, inc=1, device_id=(sp, partner), device_id_type=MESH)
+
+    def greet(target):
+        pl.semaphore_signal(barrier, inc=1, device_id=(sp, target), device_id_type=MESH)
+
+    for k, t in enumerate(chip_peers, 1):
+        opposite = ((z == 0) & (k == half - 1)) | ((z == half - 1) & (k == 1))
+        if ends:
+            pl.when(jnp.logical_not(opposite))(functools.partial(greet, t))
+        else:
+            greet(t)
     for s in sp_peers:
         pl.semaphore_signal(barrier, inc=1, device_id=(s, tp), device_id_type=MESH)
-    pl.semaphore_wait(barrier, half + n_sp - 1)
+    pl.semaphore_wait(barrier, half + n_sp - 1 - ends * at_end.astype(jnp.int32))
 
     def remote(src, dst, send, recv, device):
         return pltpu.make_async_remote_copy(
@@ -170,8 +182,9 @@
             begin(x_copy(layer, part, tp, sem, tp - 2 * k), left)
 
     def x_finish(layer, part):
+        near = 1 - 2 * ((2 * z) // half)
         for k in range(1, half):
-            slot = lax.rem(tp + 2 * k, n_tp)
+            slot = lax.rem(tp + n_tp + 2 * k * near, n_tp)
             relay = xl_sem.at[layer, part, slot]
             x_copy(layer, part, slot, relay, partner).wait_recv()
             right = x_copy(layer, part, slot, relay, tp + 2)
@@ -180,7 +193,7 @@
             begin(left, (slot > tp + 3) & (z == 1))
             begin(x_copy(layer, part, slot, xf_sem.at[layer, part, slot], partner))
         for k in range(half):
-            slot = lax.rem(partner + 2 * k, n_tp)
+            slot = lax.rem(partner + n_tp + 2 * k * near, n_tp)
             x_copy(layer, part, slot, xf_sem.at[layer, part, slot], partner).wait_recv()
 
     def w_copy(layer, which, slot, index, target):
@@ -246,27 +259,41 @@
         )
         dst[pl.ds(offset + part * chunk, chunk), :] = made.astype(jnp.bfloat16)
 
-    def attend(layer, index):
-        row = sp * rows_dev + index
-        first = jnp.minimum(jnp.maximum(row - HALO, 0), total_rows - WIN_R)
-        local = first - sp * rows_dev + HALO
-        base = first - row + WIN_R - 1
-        at = pl.ds(pl.multiple_of(local * GRID_W, GRID_W), WIN_R * GRID_W)
-        keys = kvp[layer][at, 0:feat]
-        values = kvp[layer][at, feat : 2 * feat]
-        query = q_buf[index * GRID_W : (index + 1) * GRID_W, :]
-        scores = lax.dot_general(
-            query, keys, (((1,), (1,)), ((), ())), preferred_element_type=jnp.float32
-        )
-        bias = jnp.concatenate([tiles[layer][base + 2 * j] for j in range(WIN_R // 2)], axis=1)
-        scores = scores * factor + bias
-        top = jnp.max(scores, axis=-1, keepdims=True)
-        weight = jnp.exp(scores - top)
-        weight = weight * (1.0 / jnp.sum(weight, axis=-1, keepdims=True))
-        out = jnp.dot(weight.astype(jnp.bfloat16), values, preferred_element_type=jnp.float32)
-        start = place(layer, index // group) + index % group * GRID_W
-        wide = xg[layer][tp, pl.ds(start, GRID_W), :].astype(jnp.float32)
-        return (wide + out).astype(jnp.bfloat16)
+    def attend(layer, indices):
+        places, scores = [], []
+        for index in indices:
+            row = sp * rows_dev + index
+            first = jnp.minimum(jnp.maximum(row - HALO, 0), total_rows - WIN_R)
+            local = first - sp * rows_dev + HALO
+            base = first - row + WIN_R - 1
+            at = pl.ds(pl.multiple_of(local * GRID_W, GRID_W), WIN_R * GRID_W)
+            query = q_buf[index * GRID_W : (index + 1) * GRID_W, :]
+            raw = lax.dot_general(
+                query,
+                kvp[layer][at, 0:feat],
+                (((1,), (1,)), ((), ())),
+                preferred_element_type=jnp.float32,
+            )
+            bias = jnp.concatenate([tiles[layer][base + 2 * j] for j in range(WIN_R // 2)], axis=1)
+            places.append(at)
+            scores.append(raw * factor + bias)
+        tops = [jnp.max(score, axis=-1, keepdims=True) for score in scores]
+        weights = [jnp.exp(score - top) for score, top in zip(scores, tops)]
+        scales = [1.0 / jnp.sum(weight, axis=-1, keepdims=True) for weight in weights]
+        outs = [
+            jnp.dot(
+                (weight * scale).astype(jnp.bfloat16),
+                kvp[layer][at, feat : 2 * feat],
+                preferred_element_type=jnp.float32,
+            )
+            for weight, scale, at in zip(weights, scales, places)
+        ]
+        made = []
+        for index, out in zip(indices, outs):
+            start = place(layer, index // group) + index % group * GRID_W
+            wide = xg[layer][tp, pl.ds(start, GRID_W), :].astype(jnp.float32)
+            made.append((wide + out).astype(jnp.bfloat16))
+        return made
 
     for load, part in zip(loads, orders[0]):
         load.wait()
@@ -319,12 +346,14 @@
             if wait is False:
                 pl.when(has_next)(up(layer).wait_recv)
             for index in rows:
-                made = attend(layer, index)
+                if (index - rows[0]) % BATCH == 0:
+                    batch = [i for i in rows if index <= i < index + BATCH]
+                    results = dict(zip(batch, attend(layer, batch)))
                 here = pl.ds(index * GRID_W, GRID_W)
                 if layer == 1:
-                    out_ref[here, :] = made
+                    out_ref[here, :] = results[index]
                     continue
-                xg_b[tp, here, :] = made
+                xg_b[tp, here, :] = results[index]
                 finished.add(index)
                 part = index // group
                 if all(part * group + i in finished for i in range(group)):

time: 43.2 us -> 41.3 us (0.956)
  Pallas kernels: 42.3 us -> 40.5 us
    pallas_call x1, Pallas kernels: 42.3 us -> 40.5 us  [body(): pl.pallas_call(functools.partial(kernel, n_sp, n_tp), out_shape=pltpu.VME...]
where the time goes in v4:
time: 41.3 us; the launch traced here: 41.1 us
  Pallas kernels  40.5 us (98%)
  local copies, waits for them, and re-layouts  0.66 us (2%)
    pallas_call x1, Pallas kernels, body(): pl.pallas_call(functools.partial(kernel, n_sp, n_tp), out_shape=pltpu.VME...  40.5 us

profile of v4, /device:TPU:5, one launch (start us, length us, event | category | flops | bytes accessed | tf_op | source)
XLA Modules:
  0.0 41.1 jit_solution(1022587538571537198)
XLA Ops:
  0.0 40.5 %shard_map.109 = bf16[512,128]{1,0:T(8,128)(2,1)S(1)} custom-call(bf16[512,128]{1,0:T(8,128)(2,1)} %x_ref.1, bf16[1,128]{1,0:T(2,128)(2,1)} %bitcast.6, bf16[1,128]{1,0:T(2,128)(2,1)} %bitcast.7, bf16[256,128]{1,0:T(8,128)(2,1)} %wq_a.1, bf16[256,128]{1,0:T(8,128)(2,1)} %wk_a.1, bf16[256,128]{1,0:T(8,128)(2,1)} %wv_a.1, bf16[256,128]{1,0:T(8,128)(2,1)} %wq_b.1, ...), custom_call_target="tpu_custom_call" | custom-call | tf_op jit(solution)/shard_map/pallas_call | solution.py:382
  40.5 0.7 %copy.13 = bf16[512,128]{1,0:T(8,128)(2,1)} copy(bf16[512,128]{1,0:T(8,128)(2,1)S(1)} %shard_map.109) | data formatting | bytes 262144
